TPU v7x, 32 devices: a whole 2x2x4 slice. The times are simulated.
32 devices in a mesh: fs: 8 (over z, y), tp: 4 (over x, core).
Axes of the slice: x: 2, y: 2, z: 4, core: 2. Of those that a mesh axis runs over, the one named last changes fastest.
Arguments:
- inputs: bfloat16 [2048, 2048], P('fs', 'tp'), may hold values from -6 to 6
- cotangent: bfloat16 [2048, 2048], P('fs', 'tp'), may hold values from -8 to 8
- gate_weight: bfloat16 [2048, 5632], P('fs', 'tp'), may hold values from -0.125 to 0.125
- up_weight: bfloat16 [2048, 5632], P('fs', 'tp'), may hold values from -0.125 to 0.125
- down_weight: bfloat16 [5632, 2048], P('tp', 'fs'), may hold values from -0.078125 to 0.078125
Outputs:
- grad_inputs: bfloat16 [2048, 2048], P('fs', 'tp')
- grad_gate: float32 [2048, 5632], P('fs', 'tp')
- grad_up: float32 [2048, 5632], P('fs', 'tp')
- grad_down: float32 [5632, 2048], P('tp', 'fs')
All inputs are finite; a program needn't handle non-finite values.
Results may differ from a plain program's by a relative error of at most 0.015.
Values may be sent and summed in bfloat16 or wider, within the bound.
A program may use at most 64 MiB of HBM per device.

v0:
```python
import jax
import jax.numpy as jnp
from jax import lax
from jax.sharding import PartitionSpec as P


def contract_rows(left, right):
    return lax.dot_general(
        left, right, (((0,), (0,)), ((), ())), preferred_element_type=jnp.float32
    )


def contract_cols(left, right):
    return lax.dot_general(
        left, right, (((1,), (1,)), ((), ())), preferred_element_type=jnp.float32
    )


def per_device(inputs, cotangent, gate_weight, up_weight, down_weight):
    whole_inputs, whole_cotangent = (
        lax.all_gather(inputs, "tp", axis=1, tiled=True),
        lax.all_gather(cotangent, "tp", axis=1, tiled=True),
    )
    gate_whole, up_whole = (
        lax.all_gather(gate_weight, "fs", axis=0, tiled=True),
        lax.all_gather(up_weight, "fs", axis=0, tiled=True),
    )
    gate_pre = jnp.dot(whole_inputs, gate_whole, preferred_element_type=jnp.float32)
    up_pre = jnp.dot(whole_inputs, up_whole, preferred_element_type=jnp.float32)
    gate_sig = jax.nn.sigmoid(gate_pre)
    gate_act = gate_pre * gate_sig
    hidden = (gate_act * up_pre).astype(jnp.bfloat16)
    grad_hidden = contract_cols(
        whole_cotangent, lax.all_gather(down_weight, "fs", axis=1, tiled=True)
    )
    grad_gate_pre = (grad_hidden * up_pre * gate_sig * (1.0 + gate_pre * (1.0 - gate_sig))).astype(
        jnp.bfloat16
    )
    grad_up_pre = (grad_hidden * gate_act).astype(jnp.bfloat16)
    pre_grads = jnp.concatenate([grad_gate_pre, grad_up_pre], axis=1)
    width = gate_weight.shape[1]
    partial_sum = contract_cols(grad_gate_pre, gate_whole) + contract_cols(grad_up_pre, up_whole)
    grad_inputs = lax.psum_scatter(
        partial_sum.astype(jnp.bfloat16), "tp", scatter_dimension=1, tiled=True
    )
    expand = lax.psum_scatter(
        contract_rows(whole_inputs, pre_grads).astype(jnp.bfloat16),
        "fs",
        scatter_dimension=0,
        tiled=True,
    ).astype(jnp.float32)
    down = lax.psum_scatter(
        contract_rows(whole_cotangent, hidden).astype(jnp.bfloat16),
        "fs",
        scatter_dimension=0,
        tiled=True,
    ).astype(jnp.float32)
    grad_gate = expand[:, :width]
    grad_up = expand[:, width:]
    grad_down = down.T
    return (grad_inputs, grad_gate, grad_up, grad_down)


def solution(mesh):
    return jax.shard_map(
        per_device,
        mesh=mesh,
        in_specs=(P("fs", "tp"), P("fs", "tp"), P("fs", "tp"), P("fs", "tp"), P("tp", "fs")),
        out_specs=(P("fs", "tp"), P("fs", "tp"), P("fs", "tp"), P("tp", "fs")),
        check_vma=False,
    )
```

profile of v0, /device:TPU:13, one launch (start us, length us, event | category | flops | bytes accessed | tf_op | source)
XLA Modules:
  0.0 668.8 jit_solution(8997837980882983968)
XLA Ops:
  7.2 0.7 all-gather.10.cloned.1.call-update
  7.9 0.7 all-gather.12.cloned.1.call-update
  8.7 0.7 all-gather.14.cloned.1.call-update
  9.4 0.5 all-gather.6.cloned.1.call-update
  10.0 0.5 all-gather.8.cloned.1.call-update
  10.6 17.2 %all-gather.10.cloned.1.call-done = bf16[256,2048]{1,0:T(8,128)(2,1)} async-done(((bf16[256,512]{1,0:T(8,128)(2,1)}), bf16[256,2048]{1,0:T(8,128)(2,1)}) %all-gather.10.cloned.1.call-update) | async-done | bytes 1048592 | tf_op jit(solution)/shard_map/all_gather | solution.py:21
  27.8 90.8 %all-gather.12.cloned.1.call-done = bf16[2048,1408]{1,0:T(8,128)(2,1)} async-done(((bf16[256,1408]{1,0:T(8,128)(2,1)}), bf16[2048,1408]{1,0:T(8,128)(2,1)}) %all-gather.12.cloned.1.call-update) | async-done | bytes 5767184 | tf_op jit(solution)/shard_map/all_gather | solution.py:26
  118.6 4.8 fusion.10
  123.4 87.9 %all-gather.14.cloned.1.call-done = bf16[2048,1408]{1,0:T(8,128)(2,1)} async-done(((bf16[256,1408]{1,0:T(8,128)(2,1)}), bf16[2048,1408]{1,0:T(8,128)(2,1)}) %all-gather.14.cloned.1.call-update) | async-done | bytes 5767184 | tf_op jit(solution)/shard_map/all_gather | solution.py:25
  211.3 5.5 fusion.11
  216.8 14.6 %all-gather.6.cloned.1.call-done = bf16[256,2048]{1,0:T(8,128)(2,1)} async-done(((bf16[256,512]{1,0:T(8,128)(2,1)}), bf16[256,2048]{1,0:T(8,128)(2,1)}) %all-gather.6.cloned.1.call-update) | async-done | bytes 1048592 | tf_op jit(solution)/shard_map/all_gather | solution.py:22
  231.4 5.9 fusion
  237.4 85.4 %all-gather.8.cloned.1.call-done = bf16[1408,2048]{1,0:T(8,128)(2,1)} async-done(((bf16[1408,256]{1,0:T(8,128)(2,1)}), bf16[1408,2048]{1,0:T(8,128)(2,1)}) %all-gather.8.cloned.1.call-update) | async-done | bytes 5767184 | tf_op jit(solution)/shard_map/all_gather | solution.py:34
  322.8 5.6 multiply_convert_fusion.1
  328.4 6.1 convert_bitcast_fusion
  334.7 4.9 fusion.12
  339.6 5.5 fusion.1
  345.2 92.9 %reduce-scatter.8.cloned.1.call-done = bf16[256,1408]{0,1:T(8,128)(2,1)} async-done(((bf16[2048,1408]{0,1:T(8,128)(2,1)}), bf16[256,1408]{0,1:T(8,128)(2,1)}) %reduce-scatter.8.cloned.1.call-update) | async-done | bytes 720912 | tf_op jit(solution)/shard_map/reduce_scatter | solution.py:52
  438.1 2.3 convert_bitcast_fusion.1
  440.4 192.7 %reduce-scatter.6.cloned.1.call-done = bf16[256,2816]{0,1:T(8,128)(2,1)} async-done(((bf16[2048,2816]{0,1:T(8,128)(2,1)}), bf16[256,2816]{0,1:T(8,128)(2,1)}) %reduce-scatter.6.cloned.1.call-update) | async-done | bytes 1441808 | tf_op jit(solution)/shard_map/reduce_scatter | solution.py:46
  633.1 1.5 fusion.9
  634.7 1.5 copy.10
  636.2 1.5 copy.9
  637.8 24.2 %reduce-scatter.4.cloned.1.call-done = bf16[256,512]{1,0:T(8,128)(2,1)} async-done(((bf16[256,2048]{1,0:T(8,128)(2,1)}), bf16[256,512]{1,0:T(8,128)(2,1)}) %reduce-scatter.4.cloned.1.call-update) | async-done | bytes 262160 | tf_op jit(solution)/shard_map/reduce_scatter | solution.py:43
  (17 shorter events, 0.6 us)
Async XLA Ops:
  7.2 20.6 %all-gather.10.cloned.1.call-start = ((), (), s32[]{:S(2)}) async-start(), calls=%async_computation.5 | async-start | bytes 1310720 | tf_op jit(solution)/shard_map/all_gather | solution.py:21
  7.9 110.7 %all-gather.12.cloned.1.call-start = ((), (), s32[]{:S(2)}) async-start(), calls=%async_computation.6 | async-start | bytes 6488064 | tf_op jit(solution)/shard_map/all_gather | solution.py:26
  8.6 202.6 %all-gather.14.cloned.1.call-start = ((), (), s32[]{:S(2)}) async-start(), calls=%async_computation.7 | async-start | bytes 6488064 | tf_op jit(solution)/shard_map/all_gather | solution.py:25
  9.4 222.0 %all-gather.6.cloned.1.call-start = ((), (), s32[]{:S(2)}) async-start(), calls=%async_computation.3 | async-start | bytes 1310720 | tf_op jit(solution)/shard_map/all_gather | solution.py:22
  10.0 312.8 %all-gather.8.cloned.1.call-start = ((), (), s32[]{:S(2)}) async-start(), calls=%async_computation.4 | async-start | bytes 6488064 | tf_op jit(solution)/shard_map/all_gather | solution.py:34
  10.5 427.5 %reduce-scatter.8.cloned.1.call-start = ((), (), s32[]{:S(2)}) async-start(), calls=%async_computation.10 | async-start | bytes 6488064 | tf_op jit(solution)/shard_map/reduce_scatter | solution.py:52
  27.8 183.5 %copy-start = (bf16[256,2048]{1,0:T(8,128)(2,1)S(1)}, bf16[256,2048]{1,0:T(8,128)(2,1)}, u32[]{:S(2)}) copy-start(bf16[256,2048]{1,0:T(8,128)(2,1)} %all-gather.10.cloned.1.call-done) | copy-start | bytes 3145732
  123.3 108.0 %copy-start.2 = (f32[256,1408]{1,0:T(8,128)}, f32[256,1408]{1,0:T(8,128)S(1)}, u32[]{:S(2)}) copy-start(f32[256,1408]{1,0:T(8,128)S(1)} %fusion.10) | copy-start | bytes 4325380
  237.3 85.5 %copy-start.1 = (bf16[256,2048]{1,0:T(8,128)(2,1)S(1)}, bf16[256,2048]{1,0:T(8,128)(2,1)}, u32[]{:S(2)}) copy-start(bf16[256,2048]{1,0:T(8,128)(2,1)} %all-gather.6.cloned.1.call-done) | copy-start | bytes 3145732
  237.3 395.8 %reduce-scatter.6.cloned.1.call-start = ((), (), s32[]{:S(2)}) async-start(), calls=%async_computation.9 | async-start | bytes 12976128 | tf_op jit(solution)/shard_map/reduce_scatter | solution.py:46
  334.4 327.5 %reduce-scatter.4.cloned.1.call-start = ((), (), s32[]{:S(2)}) async-start(), calls=%async_computation.8 | async-start | bytes 1310720 | tf_op jit(solution)/shard_map/reduce_scatter | solution.py:43
Sparse Core Ops, SparseCore 0:
  9.5 18.1 all-gather.9
  29.9 88.5 all-gather.11
  120.8 90.4 all-gather.13
  212.7 18.6 all-gather.5
  233.3 89.4 all-gather.7
  326.3 111.7 reduce-scatter.7
  441.7 191.3 reduce-scatter.5
  636.2 25.6 reduce-scatter.3
where the time goes:
time: 671 us; the launch traced here: 669 us
  waiting for transfers between devices  609 us (91%)
  matrix products  38.3 us (6%)
  between operations  14.2 us (2%)
    reduce_scatter x1, waiting for transfers between devices, per_device(): lax.psum_scatter(contract_rows(whole_inputs, pre_grads).astype(jnp.bfloat...  193 us
    reduce_scatter x1, waiting for transfers between devices, per_device(): lax.psum_scatter(contract_rows(whole_cotangent, hidden).astype(jnp.bfloat...  92.9 us
    all_gather x1, waiting for transfers between devices, per_device(): lax.all_gather(up_weight, 'fs', axis=0, tiled=True)  90.8 us
    all_gather x1, waiting for transfers between devices, per_device(): lax.all_gather(gate_weight, 'fs', axis=0, tiled=True)  87.9 us
    all_gather x1, waiting for transfers between devices, per_device(): lax.all_gather(down_weight, 'fs', axis=1, tiled=True)  85.4 us
    reduce_scatter x1, waiting for transfers between devices, per_device(): lax.psum_scatter(partial_sum.astype(jnp.bfloat16), 'tp', scatter_dimensio...  24.2 us
    all_gather x1, waiting for transfers between devices, per_device(): lax.all_gather(inputs, 'tp', axis=1, tiled=True)  17.2 us
    dot_general x3, matrix products, contract_cols(): lax.dot_general(left, right, (((1,), (1,)), ((), ())), preferred_element_...  16 us
  transfers between devices with their start and end apart: 8, of which 8 were waited for; matrix products, arithmetic and copies ran while one was open for 7% of the time, Pallas kernels for 0%

commit v1 on v0

v1 whole, which is shorter than its diff:
```python
import functools

import jax
import jax.numpy as jnp
from jax import lax
from jax.experimental import pallas as pl
from jax.experimental.pallas import tpu as pltpu
from jax.sharding import PartitionSpec as P

MESH = pl.DeviceIdType.MESH
ANY = pl.BlockSpec(memory_space=pl.ANY)
VMEM = pl.BlockSpec(memory_space=pltpu.VMEM)
CORES = 2


def contract_rows(left, right):
    return lax.dot_general(
        left, right, (((0,), (0,)), ((), ())), preferred_element_type=jnp.float32
    )


def contract_cols(left, right):
    return lax.dot_general(
        left, right, (((1,), (1,)), ((), ())), preferred_element_type=jnp.float32
    )


def gathered_plan(inputs, cotangent, gate_weight, up_weight, down_weight):
    whole_inputs = lax.all_gather(inputs, "tp", axis=1, tiled=True)
    whole_cotangent = lax.all_gather(cotangent, "tp", axis=1, tiled=True)
    gate_whole = lax.all_gather(gate_weight, "fs", axis=0, tiled=True)
    up_whole = lax.all_gather(up_weight, "fs", axis=0, tiled=True)
    down_whole = lax.all_gather(down_weight, "fs", axis=1, tiled=True)
    gate_pre = jnp.dot(whole_inputs, gate_whole, preferred_element_type=jnp.float32)
    up_pre = jnp.dot(whole_inputs, up_whole, preferred_element_type=jnp.float32)
    grad_hidden = contract_cols(whole_cotangent, down_whole)
    hidden, grad_gate_pre, grad_up_pre = pointwise(gate_pre, up_pre, grad_hidden)
    pre_grads = jnp.concatenate([grad_gate_pre, grad_up_pre], axis=1)
    width = gate_weight.shape[1]
    partial_sum = contract_cols(grad_gate_pre, gate_whole) + contract_cols(grad_up_pre, up_whole)

    def scattered(values, axis, dim):
        return lax.psum_scatter(
            values.astype(jnp.bfloat16), axis, scatter_dimension=dim, tiled=True
        )

    grad_inputs = scattered(partial_sum, "tp", 1)
    expand = scattered(contract_rows(whole_inputs, pre_grads), "fs", 0).astype(jnp.float32)
    down = scattered(contract_rows(whole_cotangent, hidden), "fs", 0).astype(jnp.float32)
    return (grad_inputs, expand[:, :width], expand[:, width:], down.T)


def pointwise(gate_pre, up_pre, grad_hidden):
    gate_sig = jax.nn.sigmoid(gate_pre)
    gate_act = gate_pre * gate_sig
    hidden = (gate_act * up_pre).astype(jnp.bfloat16)
    grad_gate_pre = (grad_hidden * up_pre * gate_sig * (1.0 + gate_pre * (1.0 - gate_sig))).astype(
        jnp.bfloat16
    )
    grad_up_pre = (grad_hidden * gate_act).astype(jnp.bfloat16)
    return hidden, grad_gate_pre, grad_up_pre


def block(index, size):
    return pl.ds(pl.multiple_of(index * size, size), size)


class Place:
    def __init__(self, nz, ny, nx):
        self.nz, self.ny, self.nx = nz, ny, nx
        fs, tp = lax.axis_index("fs"), lax.axis_index("tp")
        self.fs, self.tp = fs, tp
        self.z, self.y = fs // ny, fs % ny
        self.x, self.c = tp // CORES, tp % CORES

    def by_z(self, dz):
        return {"fs": ((self.z + dz) % self.nz) * self.ny + self.y, "tp": self.tp}

    def by_y(self, dy):
        return {"fs": self.z * self.ny + (self.y + dy) % self.ny, "tp": self.tp}

    def by_x(self, dx):
        return {"fs": self.fs, "tp": ((self.x + dx) % self.nx) * CORES + self.c}

    def by_core(self):
        return {"fs": self.fs, "tp": self.x * CORES + 1 - self.c}

    def by_tp(self, dt):
        return {"fs": self.fs, "tp": (self.tp + dt) % (self.nx * CORES)}


def meet(partners):
    barrier = pltpu.get_barrier_semaphore()
    for partner in partners:
        pl.semaphore_signal(barrier, inc=1, device_id=partner, device_id_type=MESH)
    pl.semaphore_wait(barrier, len(partners))


class Copies:
    def __init__(self, send_sem, recv_sem):
        self.send_sem, self.recv_sem, self.made = send_sem, recv_sem, []

    def start(self, source, target, device):
        at = len(self.made)
        copy = pltpu.make_async_remote_copy(
            src_ref=source, dst_ref=target, send_sem=self.send_sem.at[at],
            recv_sem=self.recv_sem.at[at], device_id=device, device_id_type=MESH,
        )
        copy.start()
        self.made.append(copy)
        return copy


def gather_kernel(sizes, x_ref, c_ref, w_ref, xf, cf, wf, send_sem, recv_sem, own_sem):
    nz, ny, nx = sizes
    me = Place(*sizes)
    tokens, features = x_ref.shape
    depth = w_ref.shape[3]
    meet(
        [me.by_z(d) for d in range(1, nz)]
        + [me.by_y(d) for d in range(1, ny)]
        + [me.by_x(d) for d in range(1, nx)]
        + [me.by_core()]
    )
    copies = Copies(send_sem, recv_sem)
    pairs = ((x_ref, xf), (c_ref, cf))

    def spot(whole, dz, tp):
        return whole.at[block((me.z - dz + nz) % nz, tokens), block(tp, features)]

    def w_spot(dz):
        return wf.at[:, :, block(((me.z - dz + nz) % nz) * ny + me.y, depth)]

    own = []
    for at, (source, target) in enumerate(
        [(source, spot(whole, 0, me.tp)) for source, whole in pairs]
        + [(w_ref.at[me.z], w_spot(0))]
    ):
        own.append(pltpu.make_async_copy(source, target, own_sem.at[at]))
        own[-1].start()
    across = {}
    sent_z = [
        [copies.start(source, spot(whole, 0, me.tp), me.by_z(dz)) for source, whole in pairs]
        for dz in range(1, nz)
    ]
    for dx in range(1, nx):
        across[0, dx] = [
            copies.start(source, spot(whole, 0, me.tp), me.by_x(dx)) for source, whole in pairs
        ]
    last = [copies.start(source, spot(whole, 0, me.tp), me.by_core()) for source, whole in pairs]
    w_sent = [
        copies.start(w_ref.at[(me.z + dz) % nz], w_spot(0), me.by_z(dz)) for dz in range(1, nz)
    ]
    last += [copies.start(w_ref.at[me.z], w_spot(0), me.by_y(dy)) for dy in range(1, ny)]
    for dz in range(1, nz):
        for copy in sent_z[dz - 1]:
            copy.wait_recv()
        for dx in range(1, nx):
            across[dz, dx] = [
                copies.start(spot(whole, dz, me.tp), spot(whole, dz, me.tp), me.by_x(dx))
                for _, whole in pairs
            ]
        last += [
            copies.start(spot(whole, dz, me.tp), spot(whole, dz, me.tp), me.by_core())
            for _, whole in pairs
        ]
    for dz in range(nz):
        if dz:
            w_sent[dz - 1].wait_recv()
            last += [copies.start(w_spot(dz), w_spot(dz), me.by_y(dy)) for dy in range(1, ny)]
        for dx in range(1, nx):
            for copy in across[dz, dx]:
                copy.wait_recv()
            tp = ((me.x - dx + nx) % nx) * CORES + me.c
            last += [
                copies.start(spot(whole, dz, tp), spot(whole, dz, tp), me.by_core())
                for _, whole in pairs
            ]
    for copy in last:
        copy.wait_recv()
    for copy in copies.made:
        copy.wait_send()
    for copy in own:
        copy.wait()


def spread_kernel(sizes, g_ref, i_ref, rg, ri, send_sem, recv_sem):
    nz, ny, nx = sizes
    me = Place(*sizes)
    n_tp = nx * CORES
    depth, features = rg.shape[3] // nz, ri.shape[2]
    meet([me.by_y(d) for d in range(1, ny)] + [me.by_tp(d) for d in range(1, n_tp)])
    copies = Copies(send_sem, recv_sem)
    for dy in range(1, ny):
        for z in range(nz):
            copies.start(
                g_ref.at[:, :, block(z * ny + (me.y + dy) % ny, depth)],
                rg.at[dy - 1, :, :, pl.ds(z * depth, depth)],
                me.by_y(dy),
            )
    for dt in range(1, n_tp):
        copies.start(
            i_ref.at[:, block((me.tp + dt) % n_tp, features)], ri.at[dt - 1], me.by_tp(dt)
        )
    for copy in copies.made:
        copy.wait()


def settle_kernel(sizes, s_ref, i_ref, r, rz, send_sem, recv_sem, own_sem):
    nz, _, _ = sizes
    me = Place(*sizes)
    depth, tokens, units = s_ref.shape[2] // nz, rz.shape[1], s_ref.shape[1]
    meet([me.by_z(d) for d in range(1, nz)])
    target = r.at[:, block(me.z, units), :]
    own = pltpu.make_async_copy(s_ref.at[:, :, block(me.z, depth)], target, own_sem)
    own.start()
    copies = Copies(send_sem, recv_sem)
    for dz in range(1, nz):
        there = (me.z + dz) % nz
        copies.start(s_ref.at[:, :, block(there, depth)], target, me.by_z(dz))
        copies.start(i_ref.at[block(there, tokens), :], rz.at[dz - 1], me.by_z(dz))
    for copy in copies.made:
        copy.wait()
    own.wait()


def call(kernel, sizes, shapes, in_specs, count, own, identity, *operands):
    semaphores = [pltpu.SemaphoreType.DMA((count,)), pltpu.SemaphoreType.DMA((count,))]
    return pl.pallas_call(
        functools.partial(kernel, sizes),
        out_shape=[jax.ShapeDtypeStruct(shape, jnp.bfloat16) for shape in shapes],
        in_specs=in_specs,
        out_specs=[ANY] * len(shapes),
        scratch_shapes=semaphores + own,
        compiler_params=pltpu.CompilerParams(collective_id=identity, has_side_effects=True),
    )(*operands)


def split_plan(sizes, inputs, cotangent, gate_weight, up_weight, down_weight):
    nz, ny, nx = sizes
    n_tp = nx * CORES
    tokens, features = inputs.shape
    depth, width = gate_weight.shape
    units, rows, model = width // nz, tokens * nz, depth * nz * ny
    here_z = lax.axis_index("fs") // ny
    here_y = lax.axis_index("fs") % ny
    here_tp = lax.axis_index("tp")
    weights = jnp.stack(
        [
            gate_weight.T.reshape(nz, units, depth),
            up_weight.T.reshape(nz, units, depth),
            down_weight.reshape(nz, units, depth),
        ],
        axis=1,
    )
    count = 2 * (nz * (nx - 1) + nz * nx + nz - 1) + nz - 1 + nz * (ny - 1)
    all_x, all_c, all_w = call(
        gather_kernel, sizes, [(rows, model), (rows, model), (3, units, model)],
        [VMEM] * 3, count, [pltpu.SemaphoreType.DMA((3,))], 0, inputs, cotangent, weights,
    )
    gate_pre = contract_cols(all_x, all_w[0])
    up_pre = contract_cols(all_x, all_w[1])
    grad_hidden = contract_cols(all_c, all_w[2])
    hidden, grad_gate_pre, grad_up_pre = pointwise(gate_pre, up_pre, grad_hidden)
    partial = jnp.dot(grad_gate_pre, all_w[0], preferred_element_type=jnp.float32) + jnp.dot(
        grad_up_pre, all_w[1], preferred_element_type=jnp.float32
    )
    partial = partial.astype(jnp.bfloat16)
    grads = jnp.stack(
        [
            contract_rows(grad_gate_pre, all_x).astype(jnp.bfloat16),
            contract_rows(grad_up_pre, all_x).astype(jnp.bfloat16),
            contract_rows(hidden, all_c).astype(jnp.bfloat16),
        ]
    )
    from_y, from_tp = call(
        spread_kernel, sizes, [(ny - 1, 3, units, nz * depth), (n_tp - 1, rows, features)],
        [ANY] * 2, nz * (ny - 1) + n_tp - 1, [], 1, grads, partial,
    )
    mine = lax.dynamic_index_in_dim(
        grads.reshape(3, units, nz, ny, depth), here_y, 3, keepdims=False
    ).reshape(3, units, nz * depth)
    summed = mine.astype(jnp.float32) + from_y.astype(jnp.float32).sum(0)
    part = lax.dynamic_slice_in_dim(partial, here_tp * features, features, 1)
    part = part.astype(jnp.float32) + from_tp.astype(jnp.float32).sum(0)
    part = part.astype(jnp.bfloat16)
    settled, from_z = call(
        settle_kernel, sizes, [(3, width, depth), (nz - 1, tokens, features)],
        [VMEM] * 2, 2 * (nz - 1), [pltpu.SemaphoreType.DMA], 2,
        summed.astype(jnp.bfloat16), part,
    )
    own = lax.dynamic_slice_in_dim(part, here_z * tokens, tokens, 0)
    grad_inputs = own.astype(jnp.float32) + from_z.astype(jnp.float32).sum(0)
    return (
        grad_inputs.astype(jnp.bfloat16),
        settled[0].T.astype(jnp.float32),
        settled[1].T.astype(jnp.float32),
        settled[2].astype(jnp.float32),
    )


def solution(mesh):
    n_fs, n_tp = mesh.shape["fs"], mesh.shape["tp"]
    nx = max(1, n_tp // CORES)
    ny = nx
    nz = n_fs // ny

    def per_device(inputs, cotangent, gate_weight, up_weight, down_weight):
        arrays = (inputs, cotangent, gate_weight, up_weight, down_weight)
        depth, width = gate_weight.shape
        fits = n_tp == nx * CORES and nz > 1 and ny > 1 and n_fs == nz * ny
        tiles = depth % 128 == 0 and inputs.shape[1] % 128 == 0 and inputs.shape[0] % 16 == 0
        if fits and tiles and width % (16 * nz) == 0:
            return split_plan((nz, ny, nx), *arrays)
        return gathered_plan(*arrays)

    return jax.shard_map(
        per_device,
        mesh=mesh,
        in_specs=(P("fs", "tp"), P("fs", "tp"), P("fs", "tp"), P("fs", "tp"), P("tp", "fs")),
        out_specs=(P("fs", "tp"), P("fs", "tp"), P("fs", "tp"), P("tp", "fs")),
        check_vma=False,
    )
```

time: 671 us -> 317 us (0.47)
  waiting for transfers between devices: 609 us -> 0 us
  Pallas kernels: 0 us -> 246 us
  local copies, waits for them, and re-layouts: 4.63 us -> 27 us
  other arithmetic: 2.32 us -> 21.6 us
  matrix products: 38.3 us -> 20.4 us
  between operations: 14.2 us -> 0.87 us
    reduce_scatter x3 -> x0, waiting for transfers between devices: 310 us -> none  [the longest x1 193 us: per_device(): lax.psum_scatter(contract_rows(whole_inputs, pre_grads).astype(jnp.bfloat...]
    all_gather x5 -> x0, waiting for transfers between devices: 296 us -> none  [the longest x1 90.8 us: per_device(): lax.all_gather(up_weight, 'fs', axis=0, tiled=True)]
    pallas_call x0 -> x3, Pallas kernels: none -> 246 us  [call(): pl.pallas_call(functools.partial(kernel, sizes), out_shape=[jax.ShapeDtyp...]
    convert_element_type x0 -> x5, other arithmetic: none -> 14.8 us  [the longest x1 4.4 us: split_plan(): summed.astype(jnp.bfloat16)]
    another operation x0 -> x6, local copies, waits for them, and re-layouts: none -> 12.5 us  [split_plan(): jnp.stack([contract_rows(grad_gate_pre, all_x).astype(jnp.bfloat16), cont...]
    dot_general x3, matrix products: 16 us -> 8.32 us  [contract_cols(): lax.dot_general(left, right, (((1,), (1,)), ((), ())), preferred_element_...]
    dot_general x2 -> x3, matrix products: 12 us -> 5.14 us  [contract_rows(): lax.dot_general(left, right, (((0,), (0,)), ((), ())), preferred_element_...]
  transfers between devices with their start and end apart: 8 -> 0, of which waited for: 8 -> 0; matrix products, arithmetic and copies ran while one was open for 7% -> 0% of each run, Pallas kernels for 0% -> 0%
where the time goes in v1:
time: 317 us; the launch traced here: 316 us
  Pallas kernels  246 us (78%)
  local copies, waits for them, and re-layouts  27 us (9%)
  other arithmetic  21.6 us (7%)
  matrix products  20.4 us (6%)
    pallas_call x3, Pallas kernels, call(): pl.pallas_call(functools.partial(kernel, sizes), out_shape=[jax.ShapeDtyp...  246 us
    another operation x6, local copies, waits for them, and re-layouts, split_plan(): jnp.stack([contract_rows(grad_gate_pre, all_x).astype(jnp.bfloat16), cont...  12.5 us
    dot_general x3, matrix products, contract_cols(): lax.dot_general(left, right, (((1,), (1,)), ((), ())), preferred_element_...  8.32 us

profile of v1, /device:TPU:13, one launch (start us, length us, event | category | flops | bytes accessed | tf_op | source)
XLA Modules:
  0.0 316.0 jit_solution(1682674468361323206)
XLA Ops:
  3.5 1.6 pad_maximum_fusion.1.w_ref
  5.1 108.6 %shard_map.84 = (bf16[1024,2048]{1,0:T(8,128)(2,1)}, bf16[1024,2048]{1,0:T(8,128)(2,1)}, bf16[3,352,2048]{2,1,0:T(8,128)(2,1)}) custom-call(bf16[256,512]{1,0:T(8,128)(2,1)} %x_ref.1, bf16[256,512]{1,0:T(8,128)(2,1)} %c_ref.1, bf16[4,3,352,256]{3,2,1,0:T(8,128)(2,1)} %pad_maximum_fusion.1.w_ref), custom_call_target="tpu_custom_call" | custom-call | tf_op jit(solution)/shard_map/pallas_call | solution.py:229
  113.7 4.5 %fusion.9 = f32[1024,352]{0,1:T(8,128)S(1)} fusion(bf16[1024,2048]{1,0:T(8,128)(2,1)} %get-tuple-element.13, bf16[3,352,2048]{2,1,0:T(8,128)(2,1)} %get-tuple-element.12), kind=kOutput, calls=%fused_computation.24 | convolution fusion | flops 1476395008 | bytes 7077888 | tf_op jit(solution)/shard_map/dot_general | solution.py:23
  118.8 1.8 fusion.6
  121.0 2.1 multiply_convert_fusion.1
  123.2 1.7 convolution_convert_fusion.1
  124.9 1.7 convolution_convert_fusion.2
  126.6 1.8 convolution_convert_fusion
  128.4 2.4 pad_maximum_fusion.g_ref
  130.8 2.4 fusion.4
  133.2 4.5 %add_convert_fusion.i_ref = bf16[1024,2048]{1,0:T(8,128)(2,1)} fusion(f32[1024,2048]{1,0:T(8,128)S(1)} %fusion.4, bf16[1024,352]{0,1:T(8,128)(2,1)S(1)} %get-tuple-element.22, bf16[3,352,2048]{2,1,0:T(8,128)(2,1)S(1)} %copy-done.5), kind=kOutput, calls=%fused_computation | convolution fusion | flops 1480589312 | bytes 14745600 | tf_op jit(solution)/shard_map/dot_general | solution.py:265
  137.7 52.4 %shard_map.85 = (bf16[1,3,352,1024]{3,2,1,0:T(8,128)(2,1)}, bf16[3,1024,512]{2,1,0:T(8,128)(2,1)}) custom-call(bf16[3,352,2048]{2,1,0:T(8,128)(2,1)} %pad_maximum_fusion.g_ref, bf16[1024,2048]{1,0:T(8,128)(2,1)} %add_convert_fusion.i_ref), custom_call_target="tpu_custom_call" | custom-call | tf_op jit(solution)/shard_map/pallas_call | solution.py:229
  190.1 2.6 convert_reduce_fusion
  192.7 2.7 add_convert_fusion.1.i_ref
  195.4 3.8 %stack.29 = bf16[1,352,4,2,256]{4,3,2,1,0:T(2,128)(2,1)S(1)} reshape(bf16[352,2048]{1,0:T(8,128)(2,1)} %copy-done.1) | data formatting | bytes 2883584 | tf_op jit(solution)/shard_map/stack | solution.py:269
  199.2 1.7 copy.12
  200.9 3.8 %stack.28 = bf16[1,352,4,2,256]{4,3,2,1,0:T(2,128)(2,1)S(1)} reshape(bf16[352,2048]{1,0:T(8,128)(2,1)} %copy-done) | data formatting | bytes 2883584 | tf_op jit(solution)/shard_map/stack | solution.py:269
  204.7 1.7 copy.11
  209.2 3.0 fusion.3
  212.2 6.2 %reshape.27 = f32[3,352,1024]{2,1,0:T(8,128)} reshape(f32[3,352,4,1,256]{4,2,1,0,3:T(4,128)} %fusion.3) | data formatting | bytes 8650752 | tf_op jit(solution)/shard_map/convert_element_type | solution.py:283
  218.4 4.4 %fusion.s_ref = bf16[3,352,1024]{2,1,0:T(8,128)(2,1)} fusion(f32[3,352,1024]{2,1,0:T(8,128)} %reshape.27, bf16[1,3,352,1024]{3,2,1,0:T(8,128)(2,1)S(1)} %copy-done.4), kind=kLoop, calls=%fused_computation.7 | loop fusion | flops 3244032 | bytes 8650752 | tf_op jit(solution)/shard_map/convert_element_type | solution.py:290
  222.8 85.3 %shard_map.86 = (bf16[3,1408,256]{2,1,0:T(8,128)(2,1)}, bf16[3,256,512]{2,1,0:T(8,128)(2,1)}) custom-call(bf16[3,352,1024]{2,1,0:T(8,128)(2,1)} %fusion.s_ref, bf16[1024,512]{1,0:T(8,128)(2,1)} %add_convert_fusion.1.i_ref), custom_call_target="tpu_custom_call" | custom-call | tf_op jit(solution)/shard_map/pallas_call | solution.py:229
  308.1 3.0 bitcast_convert_fusion
  314.3 1.7 add_convert_fusion.2
  (27 shorter events, 10.0 us)
Async XLA Ops:
  0.6 2.9 copy-start.7
  113.6 4.5 %copy-start.5 = (bf16[3,352,2048]{2,1,0:T(8,128)(2,1)S(1)}, bf16[3,352,2048]{2,1,0:T(8,128)(2,1)}, u32[]{:S(2)}) copy-start(bf16[3,352,2048]{2,1,0:T(8,128)(2,1)} %get-tuple-element.12) | copy-start | bytes 12976132
  113.7 5.2 %copy-start.9 = (bf16[1024,2048]{1,0:T(8,128)(2,1)S(1)}, bf16[1024,2048]{1,0:T(8,128)(2,1)}, u32[]{:S(2)}) copy-start(bf16[1024,2048]{1,0:T(8,128)(2,1)} %get-tuple-element.13) | copy-start | bytes 12582916
  118.8 2.2 copy-start.8
  124.9 3.5 %copy-start.1 = (bf16[352,2048]{1,0:T(8,128)(2,1)}, bf16[352,2048]{1,0:T(8,128)(2,1)S(1)}, u32[]{:S(2)}) copy-start(bf16[352,2048]{1,0:T(8,128)(2,1)S(1)} %convolution_convert_fusion.1) | copy-start | bytes 4325380
  126.6 1.8 copy-start
  207.4 1.4 copy-start.2
  207.4 1.8 copy-start.3
  212.2 6.2 %copy-start.4 = (bf16[1,3,352,1024]{3,2,1,0:T(8,128)(2,1)S(1)}, bf16[1,3,352,1024]{3,2,1,0:T(8,128)(2,1)}, u32[]{:S(2)}) copy-start(bf16[1,3,352,1024]{3,2,1,0:T(8,128)(2,1)} %get-tuple-element.15) | copy-start | bytes 6488068
  312.6 1.5 copy-start.6

commit v2 on v1

v2 whole, which is shorter than its diff:
```python
import functools

import jax
import jax.numpy as jnp
from jax import lax
from jax.experimental import pallas as pl
from jax.experimental.pallas import tpu as pltpu
from jax.sharding import PartitionSpec as P

MESH = pl.DeviceIdType.MESH
ANY = pl.BlockSpec(memory_space=pl.ANY)
VMEM = pl.BlockSpec(memory_space=pltpu.VMEM)
CORES = 2


def contract_rows(left, right):
    return lax.dot_general(
        left, right, (((0,), (0,)), ((), ())), preferred_element_type=jnp.float32
    )


def contract_cols(left, right):
    return lax.dot_general(
        left, right, (((1,), (1,)), ((), ())), preferred_element_type=jnp.float32
    )


def gathered_plan(inputs, cotangent, gate_weight, up_weight, down_weight):
    whole_inputs = lax.all_gather(inputs, "tp", axis=1, tiled=True)
    whole_cotangent = lax.all_gather(cotangent, "tp", axis=1, tiled=True)
    gate_whole = lax.all_gather(gate_weight, "fs", axis=0, tiled=True)
    up_whole = lax.all_gather(up_weight, "fs", axis=0, tiled=True)
    down_whole = lax.all_gather(down_weight, "fs", axis=1, tiled=True)
    gate_pre = jnp.dot(whole_inputs, gate_whole, preferred_element_type=jnp.float32)
    up_pre = jnp.dot(whole_inputs, up_whole, preferred_element_type=jnp.float32)
    grad_hidden = contract_cols(whole_cotangent, down_whole)
    hidden, grad_gate_pre, grad_up_pre = pointwise(gate_pre, up_pre, grad_hidden)
    pre_grads = jnp.concatenate([grad_gate_pre, grad_up_pre], axis=1)
    width = gate_weight.shape[1]
    partial_sum = contract_cols(grad_gate_pre, gate_whole) + contract_cols(grad_up_pre, up_whole)

    def scattered(values, axis, dim):
        return lax.psum_scatter(
            values.astype(jnp.bfloat16), axis, scatter_dimension=dim, tiled=True
        )

    grad_inputs = scattered(partial_sum, "tp", 1)
    expand = scattered(contract_rows(whole_inputs, pre_grads), "fs", 0).astype(jnp.float32)
    down = scattered(contract_rows(whole_cotangent, hidden), "fs", 0).astype(jnp.float32)
    return (grad_inputs, expand[:, :width], expand[:, width:], down.T)


def pointwise(gate_pre, up_pre, grad_hidden):
    gate_sig = jax.nn.sigmoid(gate_pre)
    gate_act = gate_pre * gate_sig
    hidden = (gate_act * up_pre).astype(jnp.bfloat16)
    grad_gate_pre = (grad_hidden * up_pre * gate_sig * (1.0 + gate_pre * (1.0 - gate_sig))).astype(
        jnp.bfloat16
    )
    grad_up_pre = (grad_hidden * gate_act).astype(jnp.bfloat16)
    return hidden, grad_gate_pre, grad_up_pre


def block(index, size):
    return pl.ds(pl.multiple_of(index * size, size), size)


class Place:
    def __init__(self, nz, ny, nx):
        self.nz, self.ny, self.nx = nz, ny, nx
        fs, tp = lax.axis_index("fs"), lax.axis_index("tp")
        self.fs, self.tp = fs, tp
        self.z, self.y = fs // ny, fs % ny
        self.x, self.c = tp // CORES, tp % CORES

    def by_z(self, dz):
        return {"fs": ((self.z + dz) % self.nz) * self.ny + self.y, "tp": self.tp}

    def by_y(self, dy):
        return {"fs": self.z * self.ny + (self.y + dy) % self.ny, "tp": self.tp}

    def by_x(self, dx):
        return {"fs": self.fs, "tp": ((self.x + dx) % self.nx) * CORES + self.c}

    def by_core(self):
        return {"fs": self.fs, "tp": self.x * CORES + 1 - self.c}

    def by_tp(self, dt):
        return {"fs": self.fs, "tp": (self.tp + dt) % (self.nx * CORES)}


def meet(partners):
    barrier = pltpu.get_barrier_semaphore()
    for partner in partners:
        pl.semaphore_signal(barrier, inc=1, device_id=partner, device_id_type=MESH)
    pl.semaphore_wait(barrier, len(partners))


class Copies:
    def __init__(self, send_sem, recv_sem):
        self.send_sem, self.recv_sem, self.made = send_sem, recv_sem, []

    def start(self, source, target, device):
        at = len(self.made)
        copy = pltpu.make_async_remote_copy(
            src_ref=source, dst_ref=target, send_sem=self.send_sem.at[at],
            recv_sem=self.recv_sem.at[at], device_id=device, device_id_type=MESH,
        )
        copy.start()
        self.made.append(copy)
        return copy


def flip(value, mask, nz):
    bit = 1
    while bit < nz:
        if mask & bit:
            value = value + bit - 2 * bit * ((value // bit) % 2)
        bit *= 2
    return value


def far_first(nz):
    return sorted(range(1, nz), key=lambda d: -min(d, nz - d))


def gather_kernel(sizes, x_ref, c_ref, *refs):
    nz, ny, nx = sizes
    me = Place(*sizes)
    w_refs, (xf, cf, *wfs) = refs[:3], refs[3:8]
    send_sem, recv_sem, own_sem = refs[8:]
    tokens, features = x_ref.shape
    depth, units = w_refs[0].shape[1], w_refs[0].shape[0] // nz
    bits = [1 << at for at in reversed(range(nz.bit_length() - 1))]
    meet(
        [me.by_z(d) for d in range(1, nz)]
        + [me.by_y(d) for d in range(1, ny)]
        + [me.by_x(d) for d in range(1, nx)]
        + [me.by_core()]
    )
    copies = Copies(send_sem, recv_sem)
    wholes = (xf, cf)
    by_x, sent_z, w_sent, last = {}, {}, {}, []

    def spot(whole, mask, tp):
        return whole.at[block(flip(me.z, mask, nz), tokens), block(tp, features)]

    def w_spot(whole, dz):
        return whole.at[:, block(((me.z - dz + nz) % nz) * ny + me.y, depth)]

    def held(mask):
        return (x_ref, c_ref) if mask == 0 else [spot(whole, mask, me.tp) for whole in wholes]

    def pass_z(bit, mask):
        there = {"fs": flip(me.z, bit, nz) * ny + me.y, "tp": me.tp}
        sent_z[bit, mask] = [
            copies.start(source, spot(whole, mask, me.tp), there)
            for source, whole in zip(held(mask), wholes)
        ]

    def pass_tp(mask):
        for dx in range(1, nx):
            by_x[mask, dx] = [
                copies.start(source, spot(whole, mask, me.tp), me.by_x(dx))
                for source, whole in zip(held(mask), wholes)
            ]
        for source, whole in zip(held(mask), wholes):
            last.append(copies.start(source, spot(whole, mask, me.tp), me.by_core()))

    def pass_core(mask):
        for dx in range(1, nx):
            tp = ((me.x - dx + nx) % nx) * CORES + me.c
            for copy, whole in zip(by_x[mask, dx], wholes):
                copy.wait_recv()
                here = spot(whole, mask, tp)
                last.append(copies.start(here, here, me.by_core()))

    def send_w(dz):
        w_sent[dz] = [
            copies.start(w.at[block((me.z + dz) % nz, units), :], w_spot(wf, 0), me.by_z(dz))
            for w, wf in zip(w_refs, wfs)
        ]

    for bit in bits:
        pass_z(bit, 0)
    pass_tp(0)
    order = far_first(nz)
    send_w(order[0])
    own = []
    for w, wf in zip(w_refs, wfs):
        mine = w.at[block(me.z, units), :]
        last += [copies.start(mine, w_spot(wf, 0), me.by_y(dy)) for dy in range(1, ny)]
        own.append((mine, w_spot(wf, 0)))
    own += [(x_ref, spot(xf, 0, me.tp)), (c_ref, spot(cf, 0, me.tp))]
    own = [pltpu.make_async_copy(*pair, own_sem.at[at]) for at, pair in enumerate(own)]
    for copy in own:
        copy.start()
    masks = [0]
    for at, bit in enumerate(bits):
        for mask in list(masks):
            for copy in sent_z[bit, mask]:
                copy.wait_recv()
            masks.append(mask + bit)
            for lower in bits[at + 1 :]:
                pass_z(lower, mask + bit)
            pass_tp(mask + bit)
        if at == 0:
            for dz in order[1:]:
                send_w(dz)
    for at, dz in enumerate(order):
        for copy, wf in zip(w_sent[dz], wfs):
            copy.wait_recv()
            here = w_spot(wf, dz)
            last += [copies.start(here, here, me.by_y(dy)) for dy in range(1, ny)]
        pass_core(masks[at])
    pass_core(masks[-1])
    for copy in last:
        copy.wait_recv()
    for copy in copies.made:
        copy.wait_send()
    for copy in own:
        copy.wait()


def reduce_kernel(sizes, *refs):
    nz, ny, nx = sizes
    me = Place(*sizes)
    n_tp = nx * CORES
    g_refs, i_ref, r, out = refs[:3], refs[3], refs[4], refs[5]
    rg, sg, ri, si, rz, send_sem, recv_sem, own_sem = refs[6:]
    units, depth = rg.shape[3:]
    tokens, features = rz.shape[1:]
    meet(
        [me.by_y(d) for d in range(1, ny)]
        + [me.by_tp(d) for d in range(1, n_tp)]
        + [me.by_z(d) for d in range(1, nz)]
    )
    copies = Copies(send_sem, recv_sem)
    order = far_first(nz) + [0]
    by_y, by_tp = {}, {}
    for dz in order:
        there = (me.z + dz) % nz
        for at, g in enumerate(g_refs):
            by_y[dz, at] = [
                copies.start(
                    g.at[:, block(there * ny + (me.y + dy) % ny, depth)],
                    rg.at[dy - 1, dz, at],
                    me.by_y(dy),
                )
                for dy in range(1, ny)
            ]
        by_tp[dz] = [
            copies.start(
                i_ref.at[block(there, tokens), block((me.tp + dt) % n_tp, features)],
                ri.at[dt - 1, dz],
                me.by_tp(dt),
            )
            for dt in range(1, n_tp)
        ]
    final, waiting = [], []

    def release():
        while waiting:
            final.append(copies.start(*waiting.pop(0)))

    for dz in order:
        there = (me.z + dz) % nz
        for at, g in enumerate(g_refs):
            total = g[:, block(there * ny + me.y, depth)].astype(jnp.float32)
            for dy, copy in enumerate(by_y[dz, at]):
                copy.wait_recv()
                total += rg[dy, dz, at].astype(jnp.float32)
            sg[dz, at] = total.astype(jnp.bfloat16)
            release()
            if dz:
                target = r.at[at, block(me.z, units), :]
                waiting.append((sg.at[dz, at], target, me.by_z(dz)))
    for dz in order:
        rows = block((me.z + dz) % nz, tokens)
        total = i_ref[rows, block(me.tp, features)].astype(jnp.float32)
        for dt, copy in enumerate(by_tp[dz]):
            copy.wait_recv()
            total += ri[dt, dz].astype(jnp.float32)
        si[dz] = total.astype(si.dtype)
        release()
        if dz:
            waiting.append((si.at[dz], rz.at[dz - 1], me.by_z(dz)))
    own = pltpu.make_async_copy(sg.at[0], r.at[:, block(me.z, units), :], own_sem)
    own.start()
    for copy in final:
        copy.wait_recv()
    total = si[0].astype(jnp.float32)
    for dz in range(1, nz):
        total += rz[dz - 1].astype(jnp.float32)
    out[...] = total.astype(out.dtype)
    for copy in copies.made:
        copy.wait_send()
    own.wait()


def split_plan(sizes, inputs, cotangent, gate_weight, up_weight, down_weight):
    nz, ny, nx = sizes
    n_tp = nx * CORES
    tokens, features = inputs.shape
    depth, width = gate_weight.shape
    units, rows, model = width // nz, tokens * nz, depth * nz * ny
    dma, half = pltpu.SemaphoreType.DMA, jnp.bfloat16
    count = 2 * (nz * (nx - 1) + nz * nx + nz - 1) + 3 * (nz - 1) + 3 * nz * (ny - 1)
    all_x, all_c, gate_whole, up_whole, down_whole = pl.pallas_call(
        functools.partial(gather_kernel, sizes),
        out_shape=[jax.ShapeDtypeStruct((rows, model), half)] * 2
        + [jax.ShapeDtypeStruct((units, model), half)] * 3,
        in_specs=[VMEM] * 5,
        out_specs=[ANY] * 5,
        scratch_shapes=[dma((count,)), dma((count,)), dma((5,))],
        compiler_params=pltpu.CompilerParams(collective_id=0, has_side_effects=True),
    )(inputs, cotangent, gate_weight.T, up_weight.T, down_weight)
    gate_pre = contract_cols(all_x, gate_whole)
    up_pre = contract_cols(all_x, up_whole)
    grad_hidden = contract_cols(all_c, down_whole)
    hidden, grad_gate_pre, grad_up_pre = pointwise(gate_pre, up_pre, grad_hidden)
    partial = jnp.dot(grad_gate_pre, gate_whole, preferred_element_type=jnp.float32) + jnp.dot(
        grad_up_pre, up_whole, preferred_element_type=jnp.float32
    )
    count = nz * (3 * (ny - 1) + n_tp - 1) + 4 * (nz - 1)
    settled, grad_inputs = pl.pallas_call(
        functools.partial(reduce_kernel, sizes),
        out_shape=[
            jax.ShapeDtypeStruct((3, width, depth), half),
            jax.ShapeDtypeStruct((tokens, features), half),
        ],
        in_specs=[VMEM] * 4,
        out_specs=[ANY, VMEM],
        scratch_shapes=[
            pltpu.VMEM((ny - 1, nz, 3, units, depth), half),
            pltpu.VMEM((nz, 3, units, depth), half),
            pltpu.VMEM((n_tp - 1, nz, tokens, features), half),
            pltpu.VMEM((nz, tokens, features), half),
            pltpu.VMEM((nz - 1, tokens, features), half),
            dma((count,)),
            dma((count,)),
            dma,
        ],
        compiler_params=pltpu.CompilerParams(collective_id=1, has_side_effects=True),
    )(
        contract_rows(grad_gate_pre, all_x).astype(half),
        contract_rows(grad_up_pre, all_x).astype(half),
        contract_rows(hidden, all_c).astype(half),
        partial.astype(half),
    )
    return (
        grad_inputs,
        settled[0].T.astype(jnp.float32),
        settled[1].T.astype(jnp.float32),
        settled[2].astype(jnp.float32),
    )


def solution(mesh):
    n_fs, n_tp = mesh.shape["fs"], mesh.shape["tp"]
    nx = max(1, n_tp // CORES)
    ny = nx
    nz = n_fs // ny

    def per_device(inputs, cotangent, gate_weight, up_weight, down_weight):
        arrays = (inputs, cotangent, gate_weight, up_weight, down_weight)
        depth, width = gate_weight.shape
        fits = n_tp == nx * CORES and nz > 1 and ny > 1 and n_fs == nz * ny
        fits = fits and nz & (nz - 1) == 0
        tiles = depth % 128 == 0 and inputs.shape[1] % 128 == 0 and inputs.shape[0] % 16 == 0
        if fits and tiles and width % (16 * nz) == 0:
            return split_plan((nz, ny, nx), *arrays)
        return gathered_plan(*arrays)

    return jax.shard_map(
        per_device,
        mesh=mesh,
        in_specs=(P("fs", "tp"), P("fs", "tp"), P("fs", "tp"), P("fs", "tp"), P("tp", "fs")),
        out_specs=(P("fs", "tp"), P("fs", "tp"), P("fs", "tp"), P("tp", "fs")),
        check_vma=False,
    )
```

time: 317 us -> 209 us (0.66)
  Pallas kernels: 246 us -> 171 us
  local copies, waits for them, and re-layouts: 27 us -> 8.15 us
  other arithmetic: 21.6 us -> 3 us
  matrix products: 20.4 us -> 23.9 us
    pallas_call x3 -> x2, Pallas kernels: 246 us -> 171 us  [the longest x1 85.7 us: split_plan(): pl.pallas_call(functools.partial(gather_kernel, sizes), out_shape=[jax.Sh...]
    another operation x6 -> x0, local copies, waits for them, and re-layouts: 12.5 us -> none  [split_plan(): jnp.stack([contract_rows(grad_gate_pre, all_x).astype(jnp.bfloat16), cont...]
    convert_element_type x4 -> x0, other arithmetic: 11.8 us -> none  [the longest x1 4.4 us: split_plan(): summed.astype(jnp.bfloat16)]
    convert_element_type x1 -> x0, local copies, waits for them, and re-layouts: 6.15 us -> none  [split_plan(): summed = mine.astype(jnp.float32) + from_y.astype(jnp.float32).sum(0)]
    another operation x2 -> x0, other arithmetic: 4.02 us -> none  [the longest x1 2.42 us: split_plan(): jnp.stack([contract_rows(grad_gate_pre, all_x).astype(jnp.bfloat16), cont...]
    dot_general x3, matrix products: 5.14 us -> 8.5 us  [contract_rows(): lax.dot_general(left, right, (((0,), (0,)), ((), ())), preferred_element_...]
    unnamed x22 -> x19, local copies, waits for them, and re-layouts: 5.45 us -> 8.15 us
where the time goes in v2:
time: 209 us; the launch traced here: 206 us
  Pallas kernels  171 us (82%)
  matrix products  23.9 us (11%)
  local copies, waits for them, and re-layouts  8.15 us (4%)
  other arithmetic  3 us (1%)
    pallas_call x1, Pallas kernels, split_plan(): pl.pallas_call(functools.partial(gather_kernel, sizes), out_shape=[jax.Sh...  85.7 us
    pallas_call x1, Pallas kernels, split_plan(): pl.pallas_call(functools.partial(reduce_kernel, sizes), out_shape=[jax.Sh...  85 us
    dot_general x3, matrix products, contract_rows(): lax.dot_general(left, right, (((0,), (0,)), ((), ())), preferred_element_...  8.5 us
    dot_general x3, matrix products, contract_cols(): lax.dot_general(left, right, (((1,), (1,)), ((), ())), preferred_element_...  8.3 us
    unnamed x19, local copies, waits for them, and re-layouts  8.15 us
    dot_general x1, matrix products, split_plan(): jnp.dot(grad_up_pre, up_whole, preferred_element_type=jnp.float32)  4.69 us

profile of v2, /device:TPU:13, one launch (start us, length us, event | category | flops | bytes accessed | tf_op | source)
XLA Modules:
  0.0 206.4 jit_solution(2690535426892039590)
XLA Ops:
  0.6 0.0 copy-start.2
  0.6 2.3 %copy.9 = bf16[256,1408]{0,1:T(8,128)(2,1)} copy(bf16[256,1408]{1,0:T(8,128)(2,1)} %param.7) | data formatting | bytes 1441792 | tf_op args[2]
  3.0 0.0 copy-done.2
  3.0 1.1 copy.10
  4.1 85.7 %shard_map.84 = (bf16[1024,2048]{1,0:T(8,128)(2,1)}, bf16[1024,2048]{1,0:T(8,128)(2,1)}, bf16[352,2048]{1,0:T(8,128)(2,1)}, bf16[352,2048]{1,0:T(8,128)(2,1)}, bf16[352,2048]{1,0:T(8,128)(2,1)}) custom-call(bf16[256,512]{1,0:T(8,128)(2,1)} %x_ref.1, bf16[256,512]{1,0:T(8,128)(2,1)} %c_ref.1, bf16[1408,256]{1,0:T(8,128)(2,1)} %bitcast.30, ...), custom_call_target="tpu_custom_call" | custom-call | tf_op jit(solution)/shard_map/pallas_call | solution.py:309
  89.8 0.0 copy-start.1
  89.8 0.0 copy-start.4
  89.8 4.5 %fusion.3 = f32[1024,352]{0,1:T(8,128)S(1)} fusion(bf16[1024,2048]{1,0:T(8,128)(2,1)} %get-tuple-element.13, bf16[352,2048]{1,0:T(8,128)(2,1)} %get-tuple-element.14), kind=kOutput, calls=%fused_computation.13 | convolution fusion | flops 1476395008 | bytes 7077888 | tf_op jit(solution)/shard_map/dot_general | solution.py:23
  94.3 0.0 copy-done.1
  94.3 0.0 copy-done.4
  94.3 1.7 fusion.4
  96.0 0.5 copy-done.5
  96.5 0.4 copy-done.6
  96.9 2.1 %multiply_convert_fusion.1 = (bf16[1024,352]{0,1:T(8,128)(2,1)S(1)}, bf16[1024,352]{0,1:T(8,128)(2,1)S(1)}) fusion(f32[1024,352]{0,1:T(8,128)S(1)} %fusion.4, f32[1024,352]{0,1:T(8,128)S(1)} %fusion.3, bf16[1024,2048]{1,0:T(8,128)(2,1)S(1)} %copy-done.5, bf16[352,2048]{1,0:T(8,128)(2,1)S(1)} %copy-done.6), kind=kOutput, calls=%fused_computation.7 | convolution fusion | flops 1481080832 | bytes 9961472 | tf_op jit(solution)/shard_map/dot_general | solution.py:23
  99.1 2.9 %convolution_convert_fusion.refs_2_ = bf16[352,2048]{1,0:T(8,128)(2,1)} fusion(bf16[1024,2048]{1,0:T(8,128)(2,1)S(1)} %copy-done.5, f32[1024,352]{0,1:T(8,128)S(1)} %fusion.3, f32[1024,352]{0,1:T(8,128)S(1)} %fusion.4), kind=kOutput, calls=%fused_computation.1 | convolution fusion | flops 1479278592 | bytes 8519680 | tf_op jit(solution)/shard_map/dot_general | solution.py:17
  102.0 2.8 %convolution_convert_fusion.1.refs_1_ = bf16[352,2048]{1,0:T(8,128)(2,1)} fusion(bf16[1024,352]{0,1:T(8,128)(2,1)S(1)} %get-tuple-element.22, bf16[1024,2048]{1,0:T(8,128)(2,1)S(1)} %copy-done.4), kind=kOutput, calls=%fused_computation.2 | convolution fusion | flops 1477115904 | bytes 6356992 | tf_op jit(solution)/shard_map/dot_general | solution.py:17
  104.8 2.8 %convolution_convert_fusion.2.refs_0_ = bf16[352,2048]{1,0:T(8,128)(2,1)} fusion(bf16[1024,352]{0,1:T(8,128)(2,1)S(1)} %get-tuple-element.23, bf16[1024,2048]{1,0:T(8,128)(2,1)S(1)} %copy-done.4), kind=kOutput, calls=%fused_computation.3 | convolution fusion | flops 1477115904 | bytes 6356992 | tf_op jit(solution)/shard_map/dot_general | solution.py:17
  107.6 2.4 %fusion.5 = f32[1024,2048]{1,0:T(8,128)S(1)} fusion(bf16[1024,352]{0,1:T(8,128)(2,1)S(1)} %get-tuple-element.23, bf16[352,2048]{1,0:T(8,128)(2,1)S(1)} %copy-done.1), kind=kOutput, calls=%fused_computation.15 | convolution fusion | flops 1476395008 | bytes 10551296 | tf_op jit(solution)/shard_map/dot_general | solution.py:322
  110.0 4.7 %add_convert_fusion.refs_3_ = bf16[1024,2048]{1,0:T(8,128)(2,1)} fusion(f32[1024,2048]{1,0:T(8,128)S(1)} %fusion.5, bf16[1024,352]{0,1:T(8,128)(2,1)S(1)} %get-tuple-element.22, bf16[352,2048]{1,0:T(8,128)(2,1)S(1)} %copy-done), kind=kOutput, calls=%fused_computation | convolution fusion | flops 1480589312 | bytes 14745600 | tf_op jit(solution)/shard_map/dot_general | solution.py:322
  114.7 85.0 %shard_map.85 = (bf16[3,1408,256]{2,1,0:T(8,128)(2,1)}, bf16[256,512]{1,0:T(8,128)(2,1)}) custom-call(bf16[352,2048]{1,0:T(8,128)(2,1)} %convolution_convert_fusion.2.refs_0_, bf16[352,2048]{1,0:T(8,128)(2,1)} %convolution_convert_fusion.1.refs_1_, bf16[352,2048]{1,0:T(8,128)(2,1)} %convolution_convert_fusion.refs_2_, bf16[1024,2048]{1,0:T(8,128)(2,1)} %add_convert_fusion.refs_3_), custom_call_target="tpu_custom_call" | custom-call | tf_op jit(solution)/shard_map/pallas_call | solution.py:326
  199.6 3.0 %bitcast_convert_fusion = (f32[1408,256]{1,0:T(8,128)}, f32[256,1408]{0,1:T(8,128)S(1)}, f32[256,1408]{0,1:T(8,128)S(1)}) fusion(bf16[3,1408,256]{2,1,0:T(8,128)(2,1)} %get-tuple-element.17), kind=kLoop, calls=%fused_computation.11 | loop fusion | flops 1081344 | bytes 6488064 | tf_op jit(solution)/shard_map/convert_element_type | solution.py:355
  202.6 1.5 copy.12
  204.2 1.5 copy.11
  205.7 0.7 copy.14
  (6 shorter events, 0.0 us)
Async XLA Ops:
  0.6 2.3 %copy-start.2 = (bf16[256,1408]{1,0:T(8,128)(2,1)S(1)}, bf16[256,1408]{1,0:T(8,128)(2,1)}, u32[]{:S(2)}) copy-start(bf16[256,1408]{1,0:T(8,128)(2,1)} %param.8) | copy-start | bytes 2162692
  89.8 4.5 %copy-start.1 = (bf16[352,2048]{1,0:T(8,128)(2,1)S(1)}, bf16[352,2048]{1,0:T(8,128)(2,1)}, u32[]{:S(2)}) copy-start(bf16[352,2048]{1,0:T(8,128)(2,1)} %get-tuple-element.15) | copy-start | bytes 4325380
  89.8 4.5 %copy-start.4 = (bf16[1024,2048]{1,0:T(8,128)(2,1)S(1)}, bf16[1024,2048]{1,0:T(8,128)(2,1)}, u32[]{:S(2)}) copy-start(bf16[1024,2048]{1,0:T(8,128)(2,1)} %get-tuple-element.13) | copy-start | bytes 12582916
  94.3 2.2 %copy-start.5 = (bf16[1024,2048]{1,0:T(8,128)(2,1)S(1)}, bf16[1024,2048]{1,0:T(8,128)(2,1)}, u32[]{:S(2)}) copy-start(bf16[1024,2048]{1,0:T(8,128)(2,1)} %get-tuple-element.11) | copy-start | bytes 12582916
  94.3 2.6 %copy-start.6 = (bf16[352,2048]{1,0:T(8,128)(2,1)S(1)}, bf16[352,2048]{1,0:T(8,128)(2,1)}, u32[]{:S(2)}) copy-start(bf16[352,2048]{1,0:T(8,128)(2,1)} %get-tuple-element.12) | copy-start | bytes 4325380
  107.6 2.4 %copy-start = (bf16[352,2048]{1,0:T(8,128)(2,1)S(1)}, bf16[352,2048]{1,0:T(8,128)(2,1)}, u32[]{:S(2)}) copy-start(bf16[352,2048]{1,0:T(8,128)(2,1)} %get-tuple-element.14) | copy-start | bytes 4325380
  204.2 1.5 copy-start.3

commit v3 on v2

--- a/solution.py
+++ b/solution.py
@@ -249,10 +249,12 @@
                 )
                 for dy in range(1, ny)
             ]
-        by_tp[dz] = [
+    masks = sorted(range(nz), key=lambda m: m % 2 == 0)
+    for mask in masks:
+        by_tp[mask] = [
             copies.start(
-                i_ref.at[block(there, tokens), block((me.tp + dt) % n_tp, features)],
-                ri.at[dt - 1, dz],
+                i_ref.at[block(flip(me.z, mask, nz), tokens), block((me.tp + dt) % n_tp, features)],
+                ri.at[dt - 1, mask],
                 me.by_tp(dt),
             )
             for dt in range(1, n_tp)
@@ -275,24 +277,39 @@
             if dz:
                 target = r.at[at, block(me.z, units), :]
                 waiting.append((sg.at[dz, at], target, me.by_z(dz)))
-    for dz in order:
-        rows = block((me.z + dz) % nz, tokens)
-        total = i_ref[rows, block(me.tp, features)].astype(jnp.float32)
-        for dt, copy in enumerate(by_tp[dz]):
-            copy.wait_recv()
-            total += ri[dt, dz].astype(jnp.float32)
-        si[dz] = total.astype(si.dtype)
-        release()
-        if dz:
-            waiting.append((si.at[dz], rz.at[dz - 1], me.by_z(dz)))
+    release()
     own = pltpu.make_async_copy(sg.at[0], r.at[:, block(me.z, units), :], own_sem)
     own.start()
+    halves, slots = {}, iter(range(nz - 1))
+
+    def send_half(bit, mask):
+        there = {"fs": flip(me.z, bit, nz) * ny + me.y, "tp": me.tp}
+        slot = next(slots)
+        halves[bit, mask - bit] = slot, copies.start(si.at[mask], rz.at[slot], there)
+
+    for mask in masks:
+        total = i_ref[block(flip(me.z, mask, nz), tokens), block(me.tp, features)]
+        total = total.astype(jnp.float32)
+        for dt, copy in enumerate(by_tp[mask]):
+            copy.wait_recv()
+            total += ri[dt, mask].astype(jnp.float32)
+        si[mask] = total.astype(si.dtype)
+    bit = 1
+    while bit < nz:
+        live = range(0, nz, bit)
+        for mask in live:
+            if mask & bit:
+                send_half(bit, mask)
+        for mask in sorted(live, key=lambda m: -(m & (2 * bit))):
+            if mask & bit == 0:
+                slot, copy = halves[bit, mask]
+                copy.wait_recv()
+                total = si[mask].astype(jnp.float32) + rz[slot].astype(jnp.float32)
+                si[mask] = total.astype(si.dtype)
+        bit *= 2
+    out[...] = si[0]
     for copy in final:
         copy.wait_recv()
-    total = si[0].astype(jnp.float32)
-    for dz in range(1, nz):
-        total += rz[dz - 1].astype(jnp.float32)
-    out[...] = total.astype(out.dtype)
     for copy in copies.made:
         copy.wait_send()
     own.wait()

time: 209 us -> 210 us (level)
  no operation moved by 1% of the time
where the time goes in v3:
time: 210 us; the launch traced here: 209 us
  Pallas kernels  173 us (82%)
  matrix products  23.9 us (11%)
  local copies, waits for them, and re-layouts  8.15 us (4%)
  other arithmetic  3 us (1%)
    pallas_call x1, Pallas kernels, split_plan(): pl.pallas_call(functools.partial(reduce_kernel, sizes), out_shape=[jax.Sh...  87.1 us
    pallas_call x1, Pallas kernels, split_plan(): pl.pallas_call(functools.partial(gather_kernel, sizes), out_shape=[jax.Sh...  85.7 us
    dot_general x3, matrix products, contract_rows(): lax.dot_general(left, right, (((0,), (0,)), ((), ())), preferred_element_...  8.5 us
    dot_general x3, matrix products, contract_cols(): lax.dot_general(left, right, (((1,), (1,)), ((), ())), preferred_element_...  8.3 us
    unnamed x19, local copies, waits for them, and re-layouts  8.15 us
    dot_general x1, matrix products, split_plan(): jnp.dot(grad_up_pre, up_whole, preferred_element_type=jnp.float32)  4.69 us

profile of v3, /device:TPU:13, one launch (start us, length us, event | category | flops | bytes accessed | tf_op | source)
XLA Modules:
  0.0 208.5 jit_solution(3560475852018606255)
XLA Ops:
  0.6 0.0 copy-start.2
  0.6 2.3 %copy.9 = bf16[256,1408]{0,1:T(8,128)(2,1)} copy(bf16[256,1408]{1,0:T(8,128)(2,1)} %param.7) | data formatting | bytes 1441792 | tf_op args[2]
  3.0 0.0 copy-done.2
  3.0 1.1 copy.10
  4.1 85.7 %shard_map.84 = (bf16[1024,2048]{1,0:T(8,128)(2,1)}, bf16[1024,2048]{1,0:T(8,128)(2,1)}, bf16[352,2048]{1,0:T(8,128)(2,1)}, bf16[352,2048]{1,0:T(8,128)(2,1)}, bf16[352,2048]{1,0:T(8,128)(2,1)}) custom-call(bf16[256,512]{1,0:T(8,128)(2,1)} %x_ref.1, bf16[256,512]{1,0:T(8,128)(2,1)} %c_ref.1, bf16[1408,256]{1,0:T(8,128)(2,1)} %bitcast.30, ...), custom_call_target="tpu_custom_call" | custom-call | tf_op jit(solution)/shard_map/pallas_call | solution.py:326
  89.8 0.0 copy-start.1
  89.8 0.0 copy-start.4
  89.8 4.5 %fusion.3 = f32[1024,352]{0,1:T(8,128)S(1)} fusion(bf16[1024,2048]{1,0:T(8,128)(2,1)} %get-tuple-element.13, bf16[352,2048]{1,0:T(8,128)(2,1)} %get-tuple-element.14), kind=kOutput, calls=%fused_computation.13 | convolution fusion | flops 1476395008 | bytes 7077888 | tf_op jit(solution)/shard_map/dot_general | solution.py:23
  94.3 0.0 copy-done.1
  94.3 1.7 fusion.4
  96.0 0.5 copy-done.5
  96.5 0.4 copy-done.6
  96.9 2.1 %multiply_convert_fusion.1 = (bf16[1024,352]{0,1:T(8,128)(2,1)S(1)}, bf16[1024,352]{0,1:T(8,128)(2,1)S(1)}) fusion(f32[1024,352]{0,1:T(8,128)S(1)} %fusion.4, f32[1024,352]{0,1:T(8,128)S(1)} %fusion.3, bf16[1024,2048]{1,0:T(8,128)(2,1)S(1)} %copy-done.5, bf16[352,2048]{1,0:T(8,128)(2,1)S(1)} %copy-done.6), kind=kOutput, calls=%fused_computation.7 | convolution fusion | flops 1481080832 | bytes 9961472 | tf_op jit(solution)/shard_map/dot_general | solution.py:23
  99.1 2.9 %convolution_convert_fusion.refs_2_ = bf16[352,2048]{1,0:T(8,128)(2,1)} fusion(bf16[1024,2048]{1,0:T(8,128)(2,1)S(1)} %copy-done.5, f32[1024,352]{0,1:T(8,128)S(1)} %fusion.3, f32[1024,352]{0,1:T(8,128)S(1)} %fusion.4), kind=kOutput, calls=%fused_computation.1 | convolution fusion | flops 1479278592 | bytes 8519680 | tf_op jit(solution)/shard_map/dot_general | solution.py:17
  102.0 2.8 %convolution_convert_fusion.1.refs_1_ = bf16[352,2048]{1,0:T(8,128)(2,1)} fusion(bf16[1024,352]{0,1:T(8,128)(2,1)S(1)} %get-tuple-element.22, bf16[1024,2048]{1,0:T(8,128)(2,1)S(1)} %copy-done.4), kind=kOutput, calls=%fused_computation.2 | convolution fusion | flops 1477115904 | bytes 6356992 | tf_op jit(solution)/shard_map/dot_general | solution.py:17
  104.8 2.8 %convolution_convert_fusion.2.refs_0_ = bf16[352,2048]{1,0:T(8,128)(2,1)} fusion(bf16[1024,352]{0,1:T(8,128)(2,1)S(1)} %get-tuple-element.23, bf16[1024,2048]{1,0:T(8,128)(2,1)S(1)} %copy-done.4), kind=kOutput, calls=%fused_computation.3 | convolution fusion | flops 1477115904 | bytes 6356992 | tf_op jit(solution)/shard_map/dot_general | solution.py:17
  107.6 2.4 %fusion.5 = f32[1024,2048]{1,0:T(8,128)S(1)} fusion(bf16[1024,352]{0,1:T(8,128)(2,1)S(1)} %get-tuple-element.23, bf16[352,2048]{1,0:T(8,128)(2,1)S(1)} %copy-done.1), kind=kOutput, calls=%fused_computation.15 | convolution fusion | flops 1476395008 | bytes 10551296 | tf_op jit(solution)/shard_map/dot_general | solution.py:339
  110.0 4.7 %add_convert_fusion.refs_3_ = bf16[1024,2048]{1,0:T(8,128)(2,1)} fusion(f32[1024,2048]{1,0:T(8,128)S(1)} %fusion.5, bf16[1024,352]{0,1:T(8,128)(2,1)S(1)} %get-tuple-element.22, bf16[352,2048]{1,0:T(8,128)(2,1)S(1)} %copy-done), kind=kOutput, calls=%fused_computation | convolution fusion | flops 1480589312 | bytes 14745600 | tf_op jit(solution)/shard_map/dot_general | solution.py:339
  114.7 87.1 %shard_map.85 = (bf16[3,1408,256]{2,1,0:T(8,128)(2,1)}, bf16[256,512]{1,0:T(8,128)(2,1)}) custom-call(bf16[352,2048]{1,0:T(8,128)(2,1)} %convolution_convert_fusion.2.refs_0_, bf16[352,2048]{1,0:T(8,128)(2,1)} %convolution_convert_fusion.1.refs_1_, bf16[352,2048]{1,0:T(8,128)(2,1)} %convolution_convert_fusion.refs_2_, bf16[1024,2048]{1,0:T(8,128)(2,1)} %add_convert_fusion.refs_3_), custom_call_target="tpu_custom_call" | custom-call | tf_op jit(solution)/shard_map/pallas_call | solution.py:343
  201.7 3.0 %bitcast_convert_fusion = (f32[1408,256]{1,0:T(8,128)}, f32[256,1408]{0,1:T(8,128)S(1)}, f32[256,1408]{0,1:T(8,128)S(1)}) fusion(bf16[3,1408,256]{2,1,0:T(8,128)(2,1)} %get-tuple-element.17), kind=kLoop, calls=%fused_computation.11 | loop fusion | flops 1081344 | bytes 6488064 | tf_op jit(solution)/shard_map/convert_element_type | solution.py:372
  204.7 1.5 copy.12
  206.3 1.5 copy.11
  207.8 0.0 copy-done.3
  207.8 0.7 copy.14
  (6 shorter events, 0.0 us)
Async XLA Ops:
  0.6 2.3 %copy-start.2 = (bf16[256,1408]{1,0:T(8,128)(2,1)S(1)}, bf16[256,1408]{1,0:T(8,128)(2,1)}, u32[]{:S(2)}) copy-start(bf16[256,1408]{1,0:T(8,128)(2,1)} %param.8) | copy-start | bytes 2162692
  89.8 4.5 %copy-start.1 = (bf16[352,2048]{1,0:T(8,128)(2,1)S(1)}, bf16[352,2048]{1,0:T(8,128)(2,1)}, u32[]{:S(2)}) copy-start(bf16[352,2048]{1,0:T(8,128)(2,1)} %get-tuple-element.15) | copy-start | bytes 4325380
  89.8 4.5 %copy-start.4 = (bf16[1024,2048]{1,0:T(8,128)(2,1)S(1)}, bf16[1024,2048]{1,0:T(8,128)(2,1)}, u32[]{:S(2)}) copy-start(bf16[1024,2048]{1,0:T(8,128)(2,1)} %get-tuple-element.13) | copy-start | bytes 12582916
  94.3 2.2 %copy-start.5 = (bf16[1024,2048]{1,0:T(8,128)(2,1)S(1)}, bf16[1024,2048]{1,0:T(8,128)(2,1)}, u32[]{:S(2)}) copy-start(bf16[1024,2048]{1,0:T(8,128)(2,1)} %get-tuple-element.11) | copy-start | bytes 12582916
  94.3 2.6 %copy-start.6 = (bf16[352,2048]{1,0:T(8,128)(2,1)S(1)}, bf16[352,2048]{1,0:T(8,128)(2,1)}, u32[]{:S(2)}) copy-start(bf16[352,2048]{1,0:T(8,128)(2,1)} %get-tuple-element.12) | copy-start | bytes 4325380
  107.6 2.4 %copy-start = (bf16[352,2048]{1,0:T(8,128)(2,1)S(1)}, bf16[352,2048]{1,0:T(8,128)(2,1)}, u32[]{:S(2)}) copy-start(bf16[352,2048]{1,0:T(8,128)(2,1)} %get-tuple-element.14) | copy-start | bytes 4325380
  206.3 1.5 copy-start.3
